TPU v7x, 256 devices: a 4x2x16 block of a 4x16x16 slice. The times are simulated.
256 devices in a mesh: grp: 2 (over y), fs: 16 (over z), tp: 8 (over x, core).
Axes of the slice: x: 4, y: 2, z: 16, core: 2. Of those that a mesh axis runs over, the one named last changes fastest.
The devices are a block of a 4x16x16 slice.
Arguments:
- incoming_representations: bfloat16 [20480, 2048], P(('grp', 'fs', 'tp')), parts along dimension 0, may hold values from -6 to 6
- perceptron_switch_coefficients: bfloat16 [2048, 5120], P('fs', 'tp'), may hold values from -0.125 to 0.125
- perceptron_expand_coefficients: bfloat16 [2048, 5120], P('fs', 'tp'), may hold values from -0.125 to 0.125
- perceptron_contract_coefficients: bfloat16 [5120, 2048], P('tp', 'fs'), may hold values from -0.5 to 0.5
- probe_coefficients: bfloat16 [2048, 512], P('fs', 'tp'), may hold values from -0.125 to 0.125
- address_coefficients: bfloat16 [2048, 512], P('fs', 'tp'), may hold values from -0.125 to 0.125
- payload_coefficients: bfloat16 [2048, 1024], P('fs', 'tp'), may hold values from -0.125 to 0.125
- emit_switch_coefficients: bfloat16 [2048, 1024], P('fs', 'tp'), may hold values from -0.125 to 0.125
- forgetting_shrink_coefficients: bfloat16 [2048, 32], replicated, may hold values from -0.125 to 0.125
- forgetting_expand_coefficients: bfloat16 [32, 512], P(None, 'tp'), may hold values from -3 to 3
- forgetting_sigmoid_intercept: float32 [512], P('tp'), may hold values from -1 to 9
- extra_forgetting_logits: float32 [20480, 512], P(('grp', 'fs'), 'tp'), parts along dimension 0, may hold values from -0.7 to 0
- subspace_rescaling_amplitude: float32 [128], replicated, may hold values from 0.1 to 1.9
- recurrence_emit_coefficients: bfloat16 [1024, 2048], P('tp', 'fs'), may hold values from -0.5 to 0.5
Outputs:
- layer_out: bfloat16 [20480, 2048], P(('grp', 'fs', 'tp')), parts along dimension 0
There are 2 independent parts, one for each index of `grp`. A program takes and returns all parts, laid end to end along the dimension named above; an argument that names none is the same for every part. Nothing has to cross between parts.
All inputs are finite; a program needn't handle non-finite values.
Results may differ from a plain program's by a relative error of at most 0.035.
Values may be sent and summed in bfloat16 or wider, within the bound.
A program may use at most 64 MiB of HBM per device.

v0:
```python
import jax
import jax.numpy as jnp
from jax import lax
from jax.sharding import PartitionSpec as P

DK = 64
DV = 128
BLOCK = 64
SEQUENCE_LENGTH = 320
residual_gain = 1.681792830507429
forgetting_steepness_multiplier = 16.0
epsilon = 1e-06


def in_order(tiles, dim):
    tiles = jnp.moveaxis(tiles, 0, dim)
    dims = tiles.shape
    return tiles.reshape(*dims[:dim], dims[dim] * dims[dim + 1], *dims[dim + 2 :])


def sent_to_all(x, axis):
    copies = jnp.broadcast_to(x, (lax.axis_size(axis), *x.shape))
    return lax.all_to_all(copies, axis, split_axis=0, concat_axis=0, tiled=True)


def collect(x, axis, dim):
    return in_order(sent_to_all(x, axis), dim)


def cut_along(x, dim, peers):
    dims = x.shape
    tiles = x.reshape(*dims[:dim], peers, dims[dim] // peers, *dims[dim + 1 :])
    return jnp.moveaxis(tiles, dim, 0)


def sent_and_summed(x, axis, dim):
    tiles = cut_along(x, dim, lax.axis_size(axis))
    arrived = lax.all_to_all(tiles, axis, split_axis=0, concat_axis=0, tiled=True)
    return arrived.astype(jnp.float32).sum(axis=0)


def in_one_piece(arrays, axis, dim, along):
    both = jnp.concatenate(arrays, axis=along)
    whole, at, done = (lax.all_gather(both, axis, axis=dim, tiled=True), 0, [])
    for a in arrays:
        done.append(lax.slice_in_dim(whole, at, at + a.shape[along], axis=along))
        at += a.shape[along]
    return tuple(done)


def post_norm(residual, branch):
    summed = residual_gain * residual.astype(jnp.float32) + branch
    average = jnp.mean(summed, axis=-1, keepdims=True)
    centred = summed - average
    variance = jnp.mean(centred * centred, axis=-1, keepdims=True)
    return (centred * lax.rsqrt(variance + epsilon)).astype(jnp.bfloat16)


def gather_group(stored):
    return collect(stored, "tp", 0)


def return_rows(hidden, weight_full):
    return sent_and_summed(
        jnp.dot(hidden, weight_full, preferred_element_type=jnp.float32).astype(jnp.bfloat16),
        "tp",
        0,
    )


def blockwise_mixing(queries, key_rows, values, forgetting_euler_power):
    token_count = queries.shape[0]
    head_count = queries.shape[1] // DK
    seq_count = token_count // SEQUENCE_LENGTH
    block_count = SEQUENCE_LENGTH // BLOCK

    def to_blocks(source, channels):
        shaped = source.astype(jnp.float32).reshape(
            seq_count, block_count, BLOCK, head_count, channels
        )
        return shaped.transpose(0, 3, 1, 2, 4)

    query_blk = to_blocks(queries, DK)
    key_blk = to_blocks(key_rows, DK)
    value_blk = to_blocks(values, DV)
    decay_blk = to_blocks(forgetting_euler_power, DK)
    inclusive = jnp.cumsum(decay_blk, axis=3)
    exclusive = inclusive - decay_blk
    block_end = inclusive[:, :, :, BLOCK - 1 :, :]
    token_positions = jnp.arange(BLOCK)
    lower_mask = (token_positions[:, None] >= token_positions[None, :])[:, :, None]
    flat_lead = seq_count * head_count * block_count

    def flatten(source):
        return source.reshape((flat_lead, BLOCK, source.shape[-1]))

    def within_block(inputs):
        query_one, key_one, value_one, incl_one, excl_one = inputs
        spread = jnp.where(
            lower_mask,
            incl_one[:, None, :] - incl_one[None, :, :],
            excl_one[None, :, :] - excl_one[:, None, :],
        )
        scores = jnp.sum(query_one[:, None, :] * key_one[None, :, :] * jnp.exp(spread), axis=-1)
        return jnp.dot(scores, value_one)

    local_out = lax.map(
        within_block,
        (
            flatten(query_blk),
            flatten(key_blk),
            flatten(value_blk),
            flatten(inclusive),
            flatten(exclusive),
        ),
    )
    local_out = local_out.reshape(value_blk.shape)
    forward_keys = key_blk * jnp.exp(block_end - inclusive)
    backward_keys = key_blk * jnp.exp(exclusive)
    forward_sums = jnp.einsum("shnld,shnlv->nshdv", forward_keys, value_blk)
    backward_sums = jnp.einsum("shnld,shnlv->nshdv", backward_keys, value_blk)
    through = jnp.moveaxis(jnp.exp(block_end[:, :, :, 0, :]), 2, 0)

    def advance(carried, inputs):
        block_sum, segment_passing_across = inputs
        return (segment_passing_across[..., None] * carried + block_sum, carried)

    start_state = jnp.zeros(forward_sums.shape[1:], jnp.float32)
    _, before = lax.scan(advance, start_state, (forward_sums, through))
    _, after = lax.scan(advance, start_state, (backward_sums, through), reverse=True)
    carried_out = jnp.einsum("shnld,nshdv->shnlv", query_blk * jnp.exp(inclusive), before)
    carried_out = carried_out + jnp.einsum(
        "shnld,nshdv->shnlv", query_blk * jnp.exp(block_end - exclusive), after
    )
    combined = local_out + carried_out
    return combined.transpose(0, 2, 3, 1, 4).reshape(token_count, head_count, DV)


def per_device(
    incoming_representations,
    perceptron_switch_coefficients,
    perceptron_expand_coefficients,
    perceptron_contract_coefficients,
    probe_coefficients,
    address_coefficients,
    payload_coefficients,
    emit_switch_coefficients,
    forgetting_shrink_coefficients,
    forgetting_expand_coefficients,
    forgetting_sigmoid_intercept,
    extra_forgetting_logits,
    subspace_rescaling_amplitude,
    recurrence_emit_coefficients,
):
    gate_full, up_full = in_one_piece(
        (perceptron_switch_coefficients, perceptron_expand_coefficients), "fs", 0, 1
    )
    down_kept = lax.all_gather(perceptron_contract_coefficients, "fs", axis=1, tiled=True)

    def expand(gathered):
        return (
            jnp.dot(gathered, gate_full, preferred_element_type=jnp.float32),
            jnp.dot(gathered, up_full, preferred_element_type=jnp.float32),
        )

    def channel_half(stored):
        gathered = gather_group(stored)
        gate_sum, up_sum = expand(gathered)
        hidden = (jax.nn.silu(gate_sum) * up_sum).astype(jnp.bfloat16)
        return post_norm(stored, 0.5 * return_rows(hidden, down_kept))

    opening_perceptron_result = channel_half(incoming_representations)
    gathered = gather_group(opening_perceptron_result)
    pieces = in_one_piece(
        (probe_coefficients, address_coefficients, payload_coefficients, emit_switch_coefficients),
        "fs",
        0,
        1,
    )
    projected = tuple(
        (jnp.dot(gathered, piece_one, preferred_element_type=jnp.float32) for piece_one in pieces)
    )
    queries, key_rows, values, outgate = [summed.astype(jnp.bfloat16) for summed in projected]
    compact_inner_dimensionality = jnp.dot(
        gathered, forgetting_shrink_coefficients, preferred_element_type=jnp.float32
    ).astype(jnp.bfloat16)
    forgetting_euler_power = (
        jax.nn.log_sigmoid(
            jnp.dot(
                compact_inner_dimensionality,
                forgetting_expand_coefficients,
                preferred_element_type=jnp.float32,
            )
            + forgetting_sigmoid_intercept
        )
        / forgetting_steepness_multiplier
        + extra_forgetting_logits
    )
    mixed_heads = blockwise_mixing(queries, key_rows, values, forgetting_euler_power)
    scaled = (
        mixed_heads
        * lax.rsqrt(jnp.mean(mixed_heads * mixed_heads, axis=-1, keepdims=True) + epsilon)
        * subspace_rescaling_amplitude
    )
    opener = jax.nn.silu(outgate.astype(jnp.float32)).reshape(mixed_heads.shape)
    gated = (scaled * opener).reshape(mixed_heads.shape[0], -1).astype(jnp.bfloat16)
    out_full = collect(recurrence_emit_coefficients, "fs", 1)
    context_blend_result = post_norm(opening_perceptron_result, return_rows(gated, out_full))
    return channel_half(context_blend_result)


def solution(mesh):
    return jax.shard_map(
        per_device,
        mesh=mesh,
        in_specs=(
            P(("grp", "fs", "tp"), None),
            P("fs", "tp"),
            P("fs", "tp"),
            P("tp", "fs"),
            P("fs", "tp"),
            P("fs", "tp"),
            P("fs", "tp"),
            P("fs", "tp"),
            P(),
            P(None, "tp"),
            P("tp"),
            P(("grp", "fs"), "tp"),
            P(),
            P("tp", "fs"),
        ),
        out_specs=P(("grp", "fs", "tp"), None),
        check_vma=False,
    )
```

profile of v0, /device:TPU:33, one launch (start us, length us, event | category | flops | bytes accessed | tf_op | source)
XLA Modules:
  0.0 500.8 jit_solution(16295634164969662825)
XLA Ops:
  6.6 1.8 pad_maximum_fusion
  10.5 54.8 %all_to_all.35 = bf16[8,80,2048]{2,1,0:T(8,128)(2,1)S(1)} all-to-all(bf16[8,80,2048]{2,1,0:T(8,128)(2,1)S(1)} %broadcast_in_dim.65), channel_id=1, replica_groups=mesh['grp'=2,'fs'=16,'tp'=8] {'tp'}, dimensions={0} | all-to-all | bytes 5242880 | tf_op jit(solution)/shard_map/all_to_all | solution.py:23
  65.3 29.9 %all-gather.4.cloned.1.call-done = bf16[2048,1280]{1,0:T(8,128)(2,1)} async-done(((bf16[128,1280]{1,0:T(8,128)(2,1)}), bf16[2048,1280]{1,0:T(8,128)(2,1)}) %all-gather.4.cloned.1.call-update) | async-done | bytes 5242896 | tf_op jit(solution)/shard_map/all_gather | solution.py:44
  95.1 5.1 %fusion.15 = f32[640,640]{1,0:T(8,128)} fusion(bf16[640,2048]{1,0:T(8,128)(2,1)S(1)} %bitcast.213, bf16[2048,1280]{1,0:T(8,128)(2,1)} %all-gather.4.cloned.1.call-done), kind=kOutput, calls=%fused_computation.35 | convolution fusion | flops 1677721600 | bytes 6881280 | tf_op jit(solution)/shard_map/dot_general | solution.py:162
  100.3 70.1 %all-gather.6.cloned.1.call-done = bf16[640,2048]{1,0:T(8,128)(2,1)} async-done(((bf16[640,128]{1,0:T(8,128)(2,1)}), bf16[640,2048]{1,0:T(8,128)(2,1)}) %all-gather.6.cloned.1.call-update) | async-done | bytes 2621456 | tf_op jit(solution)/shard_map/all_gather | solution.py:158
  170.3 12.9 %convolution_convert_fusion.1 = bf16[640,2048]{1,0:T(8,128)(2,1)} fusion(bf16[640,2048]{1,0:T(8,128)(2,1)} %all-gather.6.cloned.1.call-done, f32[640,640]{1,0:T(8,128)} %fusion.15, bf16[640,2048]{1,0:T(8,128)(2,1)S(1)} %bitcast.214, bf16[2048,1280]{1,0:T(8,128)(2,1)} %all-gather.4.cloned.1.call-done), kind=kOutput, calls=%fused_computation.27 | convolution fusion | flops 3359211520 | bytes 12124160 | tf_op jit(solution)/shard_map/dot_general | solution.py:65
  183.2 16.1 %all-to-all-start.1 = ((bf16[8,80,2048]{2,1,0:T(8,128)(2,1)}), bf16[8,80,2048]{2,1,0:T(8,128)(2,1)S(1)}, u32[]{:S(2)}, u32[]{:S(2)}) async-start(bf16[8,80,2048]{2,1,0:T(8,128)(2,1)} %bitcast.212), calls=%async_computation.1 | async-start | bytes 5242880 | tf_op jit(solution)/shard_map/all_to_all | solution.py:38
  200.4 30.8 %all-to-all-done.1 = bf16[8,80,2048]{2,1,0:T(8,128)(2,1)S(1)} async-done(((bf16[8,80,2048]{2,1,0:T(8,128)(2,1)}), bf16[8,80,2048]{2,1,0:T(8,128)(2,1)S(1)}, u32[]{:S(2)}, u32[]{:S(2)}) %all-to-all-start.1) | async-done | bytes 2621472 | tf_op jit(solution)/shard_map/all_to_all | solution.py:38
  232.3 1.9 broadcast_in_dim.67
  234.2 4.6 all-to-all-start.2
  239.0 31.8 %all-to-all-done.2 = bf16[8,80,2048]{2,1,0:T(8,128)(2,1)S(1)} async-done(((bf16[8,80,2048]{2,1,0:T(8,128)(2,1)}), bf16[8,80,2048]{2,1,0:T(8,128)(2,1)S(1)}, u32[]{:S(2)}, u32[]{:S(2)}) %all-to-all-start.2) | async-done | bytes 2621472 | tf_op jit(solution)/shard_map/all_to_all | solution.py:23
  271.7 7.1 %all-to-all-start.3 = ((bf16[16,128,128]{1,2,0:T(8,128)(2,1)}), bf16[16,128,128]{1,2,0:T(8,128)(2,1)}, u32[]{:S(2)}, u32[]{:S(2)}) async-start(bf16[16,128,128]{1,2,0:T(8,128)(2,1)} %broadcast_in_dim.69), calls=%async_computation.3 | async-start | bytes 1048576 | tf_op jit(solution)/shard_map/all_to_all | solution.py:23
  278.9 2.0 fusion.29
  281.8 2.0 fusion.28
  288.6 1.7 bitcast_subtract_fusion.3
  290.3 2.5 convolution_convert_fusion.4
  292.9 44.2 %while.41 = (s32[]{:T(128)}, f32[10,64,128]{2,1,0:T(8,128)}, f32[10,64,64]{2,1,0:T(8,128)}, f32[10,64,64]{2,1,0:T(8,128)}, f32[10,64,64]{2,1,0:T(8,128)S(1)}, /*...) while((s32[]{:T(128)}, f32[10,64,128]{2,1,0:T(8,128)}, ...), condition=%wide.region_6.7_spmd.clone, body=%wide.region_4.6_spmd.clone.sunk | while | flops 2621442 | bytes 271461 | solution.py:107
  295.8 1.5 fusion.96
  300.3 1.5 fusion.96
  304.7 1.5 fusion.96
  339.0 1.9 convolution_bitcast_fusion.2
  340.9 1.9 convolution_bitcast_fusion.1
  343.5 7.9 %while.43 = (s32[]{:T(128)}, f32[2,1,64,128]{3,2,1,0:T(8,128)S(1)}, bf16[5,2,1,64,128]{4,3,1,2,0:T(8,128)(2,1)}, f32[5,2,1,64]{3,1,2,0:T(2,128)S(1)}, f32[5,2,1,...) while((s32[]{:T(128)}, f32[2,1,64,128]{3,2,1,0:T(8,128)S(1)}, ...), condition=%wide.region_10.11_spmd.clone, body=%wide.region_9.10_spmd.clone.sunk | while | flops 65540 | bytes 296576 | solution.py:130
  352.1 7.8 %while.42 = (s32[]{:T(128)}, f32[2,1,64,128]{3,2,1,0:T(8,128)S(1)}, bf16[5,2,1,64,128]{4,3,1,2,0:T(8,128)(2,1)}, f32[5,2,1,64]{3,1,2,0:T(2,128)S(1)}, f32[5,2,1,64,128]{4,3,1,2,0:T(8,128)}, /*index=5*/s32[]{:T(128)}, s32[]{:T(128)}) while((s32[]{:T(128)}, f32[2,1,64,128]{3,2,1,0:T(8,128)S(1)}, ...), condition=%wide.region_8.9_spmd.clone, body=%wide.region_7.8_spmd.clone.sunk | while | flops 65539 | bytes 296556 | solution.py:129
  361.1 2.2 multiply_reduce_fusion.4
  363.4 2.0 fusion.42
  365.4 1.9 convolution_convert_fusion.2
  367.3 35.6 %all_to_all.36 = bf16[8,80,2048]{2,1,0:T(8,128)(2,1)S(1)} all-to-all(bf16[8,80,2048]{2,1,0:T(8,128)(2,1)S(1)} %bitcast.200), channel_id=1, replica_groups=mesh['grp'=2,'fs'=16,'tp'=8] {'tp'}, dimensions={0} | all-to-all | bytes 5242880 | tf_op jit(solution)/shard_map/all_to_all | solution.py:38
  404.2 35.5 %all_to_all.37 = bf16[8,80,2048]{2,1,0:T(8,128)(2,1)S(1)} all-to-all(bf16[8,80,2048]{2,1,0:T(8,128)(2,1)S(1)} %broadcast_in_dim.70), channel_id=1, replica_groups=mesh['grp'=2,'fs'=16,'tp'=8] {'tp'}, dimensions={0} | all-to-all | bytes 5242880 | tf_op jit(solution)/shard_map/all_to_all | solution.py:23
  439.8 3.4 fusion.13
  443.1 12.9 %convolution_convert_fusion = bf16[640,2048]{1,0:T(8,128)(2,1)} fusion(bf16[640,2048]{1,0:T(8,128)(2,1)} %all-gather.6.cloned.1.call-done, f32[640,640]{0,1:T(8,128)} %fusion.13, bf16[640,2048]{1,0:T(8,128)(2,1)S(1)} %bitcast.216, bf16[2048,1280]{1,0:T(8,128)(2,1)} %all-gather.4.cloned.1.call-done), kind=kOutput, calls=%fused_computation.26 | convolution fusion | flops 3359211520 | bytes 12124160 | tf_op jit(solution)/shard_map/dot_general | solution.py:65
  456.0 36.4 %all_to_all.38 = bf16[8,80,2048]{2,1,0:T(8,128)(2,1)S(1)} all-to-all(bf16[8,80,2048]{2,1,0:T(8,128)(2,1)} %bitcast.217), channel_id=1, replica_groups=mesh['grp'=2,'fs'=16,'tp'=8] {'tp'}, dimensions={0} | all-to-all | bytes 5242880 | tf_op jit(solution)/shard_map/all_to_all | solution.py:38
  (155 shorter events, 74.1 us)
Async XLA Ops:
  6.5 278.2 %copy-start = (bf16[2048,32]{0,1:T(8,128)(2,1)S(1)}, bf16[2048,32]{0,1:T(8,128)(2,1)}, u32[]{:S(2)}) copy-start(bf16[2048,32]{0,1:T(8,128)(2,1)} %param.28) | copy-start | bytes 393220
  6.6 88.6 %all-gather.4.cloned.1.call-start = ((), (), s32[]{:S(2)}) async-start(), calls=%async_computation.7 | async-start | bytes 5570560 | tf_op jit(solution)/shard_map/all_gather | solution.py:44
  8.4 161.9 %all-gather.6.cloned.1.call-start = ((), (), s32[]{:S(2)}) async-start(), calls=%async_computation.8 | async-start | bytes 2785280 | tf_op jit(solution)/shard_map/all_gather | solution.py:158
  183.2 16.2 %copy-start.6 = (bf16[128,64]{0,1:T(8,128)(2,1)S(1)}, bf16[128,64]{0,1:T(8,128)(2,1)}, u32[]{:S(2)}) copy-start(bf16[128,64]{0,1:T(8,128)(2,1)} %param.25) | copy-start | bytes 49156
  183.2 16.3 %copy-start.7 = (bf16[128,64]{0,1:T(8,128)(2,1)S(1)}, bf16[128,64]{0,1:T(8,128)(2,1)}, u32[]{:S(2)}) copy-start(bf16[128,64]{0,1:T(8,128)(2,1)} %param.24) | copy-start | bytes 49156
  183.2 16.4 %copy-start.3 = (bf16[128,128]{1,0:T(8,128)(2,1)S(1)}, bf16[128,128]{1,0:T(8,128)(2,1)}, u32[]{:S(2)}) copy-start(bf16[128,128]{1,0:T(8,128)(2,1)} %param.27) | copy-start | bytes 98308
  183.2 16.4 %copy-start.4 = (bf16[128,128]{1,0:T(8,128)(2,1)S(1)}, bf16[128,128]{1,0:T(8,128)(2,1)}, u32[]{:S(2)}) copy-start(bf16[128,128]{1,0:T(8,128)(2,1)} %param.26) | copy-start | bytes 98308
  183.2 48.0 %all-to-all-start.1 = ((bf16[8,80,2048]{2,1,0:T(8,128)(2,1)}), bf16[8,80,2048]{2,1,0:T(8,128)(2,1)S(1)}, u32[]{:S(2)}, u32[]{:S(2)}) async-start(bf16[8,80,2048]{2,1,0:T(8,128)(2,1)} %bitcast.212), calls=%async_computation.1 | async-start | bytes 5242880 | tf_op jit(solution)/shard_map/all_to_all | solution.py:38
  199.3 32.3 %copy-start.1 = (bf16[80,2048]{1,0:T(8,128)(2,1)S(1)}, bf16[80,2048]{1,0:T(8,128)(2,1)}, u32[]{:S(2)}) copy-start(bf16[80,2048]{1,0:T(8,128)(2,1)} %param.20) | copy-start | bytes 983044
  199.3 79.5 %all-gather.8.cloned.1.call-start = ((), (), s32[]{:S(2)}) async-start(), calls=%async_computation.9 | async-start | bytes 1671168 | tf_op jit(solution)/shard_map/all_gather | solution.py:44
  234.2 4.7 copy-start.5
  234.2 36.6 %all-to-all-start.2 = ((bf16[8,80,2048]{2,1,0:T(8,128)(2,1)}), bf16[8,80,2048]{2,1,0:T(8,128)(2,1)S(1)}, u32[]{:S(2)}, u32[]{:S(2)}) async-start(bf16[8,80,2048]{2,1,0:T(8,128)(2,1)} %broadcast_in_dim.67), calls=%async_computation.2 | async-start | bytes 5242880 | tf_op jit(solution)/shard_map/all_to_all | solution.py:23
  271.7 93.7 %all-to-all-start.3 = ((bf16[16,128,128]{1,2,0:T(8,128)(2,1)}), bf16[16,128,128]{1,2,0:T(8,128)(2,1)}, u32[]{:S(2)}, u32[]{:S(2)}) async-start(bf16[16,128,128]{1,2,0:T(8,128)(2,1)} %broadcast_in_dim.69), calls=%async_computation.3 | async-start | bytes 1048576 | tf_op jit(solution)/shard_map/all_to_all | solution.py:23
  280.8 3.9 copy-start.2
  280.8 3.9 copy-start.8
  280.8 3.9 copy-start.9
  351.4 12.0 %copy-start.10 = (f32[128]{0:T(128)S(1)}, f32[128]{0:T(128)}, u32[]{:S(2)}) copy-start(f32[128]{0:T(128)} %param.32) | copy-start | bytes 1540
  403.3 36.5 %slice-start = ((s8[5242880]{0:T(1024)(128)(4,1)}), s8[4194304]{0:T(1024)(128)(4,1)S(1)}, s32[]{:S(2)}) async-start(s8[5242880]{0:T(1024)(128)(4,1)} %bitcast.225), calls=%async_computation.10 | async-start | bytes 8388608
  403.9 35.8 %slice-start.1 = ((s8[5242880]{0:T(1024)(128)(4,1)}), s8[1048576]{0:T(1024)(128)(4,1)S(1)}, s32[]{:S(2)}) async-start(s8[5242880]{0:T(1024)(128)(4,1)} %bitcast.225), calls=%async_computation.11 | async-start | bytes 2097152
Sparse Core Ops, SparseCore 0:
  9.1 85.9 all-gather.3
  96.9 73.4 all-gather.5
  201.9 56.6 all-gather.7
where the time goes:
time: 504 us; the launch traced here: 501 us
  waiting for transfers between devices  163 us (32%)
  blocking collectives  162 us (32%)
  matrix products  67.5 us (13%)
  other arithmetic  40.3 us (8%)
  starting transfers between devices  28 us (6%)
  local copies, waits for them, and re-layouts  25.8 us (5%)
  between operations  13.4 us (3%)
    all_to_all x2, blocking collectives, sent_to_all(): return lax.all_to_all(copies, axis, split_axis=0, concat_axis=0, tiled=True)  90.3 us
    all_to_all x2, blocking collectives, sent_and_summed(): lax.all_to_all(tiles, axis, split_axis=0, concat_axis=0, tiled=True)  72 us
    all_gather x1, waiting for transfers between devices, per_device(): lax.all_gather(perceptron_contract_coefficients, 'fs', axis=1, tiled=True)  70.1 us
    all_to_all x2, waiting for transfers between devices, sent_to_all(): return lax.all_to_all(copies, axis, split_axis=0, concat_axis=0, tiled=True)  31.8 us
    all_to_all x1, waiting for transfers between devices, sent_and_summed(): lax.all_to_all(tiles, axis, split_axis=0, concat_axis=0, tiled=True)  30.8 us
    all_gather x2, waiting for transfers between devices, in_one_piece(): whole, at, done = (lax.all_gather(both, axis, axis=dim, tiled=True), 0, [])  29.9 us
    dot_general x3, matrix products, return_rows(): jnp.dot(hidden, weight_full, preferred_element_type=jnp.float32)  27.6 us
    all_to_all x1, starting transfers between devices, sent_and_summed(): lax.all_to_all(tiles, axis, split_axis=0, concat_axis=0, tiled=True)  16.1 us
  transfers between devices with their start and end apart: 6, of which 4 were waited for; matrix products, arithmetic and copies ran while one was open for 19% of the time, Pallas kernels for 0%

commit v1 on v0

--- a/solution.py
+++ b/solution.py
@@ -155,7 +155,12 @@
     gate_full, up_full = in_one_piece(
         (perceptron_switch_coefficients, perceptron_expand_coefficients), "fs", 0, 1
     )
-    down_kept = lax.all_gather(perceptron_contract_coefficients, "fs", axis=1, tiled=True)
+    down_kept = jnp.concatenate(
+        lax.all_to_all(
+            jnp.stack([perceptron_contract_coefficients] * lax.axis_size("fs")), "fs", 0, 0
+        ),
+        axis=1,
+    )
 
     def expand(gathered):
         return (

time: 504 us -> 546 us (1.083)
  waiting for transfers between devices: 163 us -> 235 us
  blocking collectives: 162 us -> 107 us
  starting transfers between devices: 28 us -> 52.3 us
  local copies, waits for them, and re-layouts: 25.8 us -> 31.4 us
    all_gather x2, waiting for transfers between devices: 29.9 us -> 142 us  [in_one_piece(): whole, at, done = (lax.all_gather(both, axis, axis=dim, tiled=True), 0, [])]
    all_gather x1 -> x0, waiting for transfers between devices: 70.1 us -> none  [per_device(): lax.all_gather(perceptron_contract_coefficients, 'fs', axis=1, tiled=True)]
    all_to_all x2 -> x1, blocking collectives: 90.3 us -> 35.5 us  [sent_to_all(): return lax.all_to_all(copies, axis, split_axis=0, concat_axis=0, tiled=True)]
    all_to_all x2 -> x3, waiting for transfers between devices: 31.8 us -> 62.7 us  [sent_to_all(): return lax.all_to_all(copies, axis, split_axis=0, concat_axis=0, tiled=True)]
    all_to_all x2 -> x3, starting transfers between devices: 11.8 us -> 36.5 us  [sent_to_all(): return lax.all_to_all(copies, axis, split_axis=0, concat_axis=0, tiled=True)]
    all_to_all x1, starting transfers between devices: 16.1 us -> 10.1 us  [sent_and_summed(): lax.all_to_all(tiles, axis, split_axis=0, concat_axis=0, tiled=True)]
    all_to_all x0 -> x1, starting transfers between devices: none -> 5.67 us  [per_device(): lax.all_to_all(jnp.stack([perceptron_contract_coefficients] * lax.axis_si...]
  transfers between devices with their start and end apart: 6 -> 7, of which waited for: 4 -> 4; matrix products, arithmetic and copies ran while one was open for 19% -> 18% of each run, Pallas kernels for 0% -> 0%
where the time goes in v1:
time: 546 us; the launch traced here: 543 us
  waiting for transfers between devices  235 us (43%)
  blocking collectives  107 us (20%)
  matrix products  63.2 us (12%)
  starting transfers between devices  52.3 us (10%)
  other arithmetic  39.2 us (7%)
  local copies, waits for them, and re-layouts  31.4 us (6%)
  between operations  13.7 us (3%)
    all_gather x2, waiting for transfers between devices, in_one_piece(): whole, at, done = (lax.all_gather(both, axis, axis=dim, tiled=True), 0, [])  142 us
    all_to_all x2, blocking collectives, sent_and_summed(): lax.all_to_all(tiles, axis, split_axis=0, concat_axis=0, tiled=True)  72 us
    all_to_all x3, waiting for transfers between devices, sent_to_all(): return lax.all_to_all(copies, axis, split_axis=0, concat_axis=0, tiled=True)  62.7 us
    all_to_all x3, starting transfers between devices, sent_to_all(): return lax.all_to_all(copies, axis, split_axis=0, concat_axis=0, tiled=True)  36.5 us
    all_to_all x1, blocking collectives, sent_to_all(): return lax.all_to_all(copies, axis, split_axis=0, concat_axis=0, tiled=True)  35.5 us
    all_to_all x1, waiting for transfers between devices, sent_and_summed(): lax.all_to_all(tiles, axis, split_axis=0, concat_axis=0, tiled=True)  30.7 us
    dot_general x3, matrix products, return_rows(): jnp.dot(hidden, weight_full, preferred_element_type=jnp.float32)  22.4 us
    dot_general x10, matrix products, within_block(): return jnp.dot(scores, value_one)  14.6 us
  transfers between devices with their start and end apart: 7, of which 4 were waited for; matrix products, arithmetic and copies ran while one was open for 18% of the time, Pallas kernels for 0%

profile of v1, /device:TPU:33, one launch (start us, length us, event | category | flops | bytes accessed | tf_op | source)
XLA Modules:
  0.0 542.9 jit_solution(3959074983749930419)
XLA Ops:
  6.6 2.8 broadcast_in_dim.65
  9.4 24.1 %all-to-all-start = ((bf16[8,80,2048]{2,1,0:T(8,128)(2,1)}), bf16[8,80,2048]{2,1,0:T(8,128)(2,1)S(1)}, u32[]{:S(2)}, u32[]{:S(2)}) async-start(bf16[8,80,2048]{2,1,0:T(8,128)(2,1)} %broadcast_in_dim.65), calls=%async_computation | async-start | bytes 5242880 | tf_op jit(solution)/shard_map/all_to_all | solution.py:23
  34.5 30.9 %all-to-all-done = bf16[8,80,2048]{2,1,0:T(8,128)(2,1)S(1)} async-done(((bf16[8,80,2048]{2,1,0:T(8,128)(2,1)}), bf16[8,80,2048]{2,1,0:T(8,128)(2,1)S(1)}, u32[]{:S(2)}, u32[]{:S(2)}) %all-to-all-start) | async-done | bytes 2621472 | tf_op jit(solution)/shard_map/all_to_all | solution.py:23
  65.4 2.0 stack.2
  67.7 5.7 %all-to-all-start.1 = ((bf16[16,640,128]{1,2,0:T(8,128)(2,1)}), bf16[16,640,128]{1,2,0:T(8,128)(2,1)S(1)}, u32[]{:S(2)}, u32[]{:S(2)}) async-start(bf16[16,640,128]{1,2,0:T(8,128)(2,1)} %stack.2), calls=%async_computation.1 | async-start | bytes 5242880 | tf_op jit(solution)/shard_map/all_to_all | solution.py:159
  73.4 141.8 %all-gather.3.cloned.1.call-done = bf16[2048,1280]{1,0:T(8,128)(2,1)} async-done(((bf16[128,1280]{1,0:T(8,128)(2,1)}), bf16[2048,1280]{1,0:T(8,128)(2,1)}) %all-gather.3.cloned.1.call-update) | async-done | bytes 5242896 | tf_op jit(solution)/shard_map/all_gather | solution.py:44
  215.2 6.0 %fusion.15 = f32[640,640]{1,0:T(8,128)} fusion(bf16[640,2048]{1,0:T(8,128)(2,1)} %bitcast.217, bf16[2048,1280]{1,0:T(8,128)(2,1)} %all-gather.3.cloned.1.call-done), kind=kOutput, calls=%fused_computation.35 | convolution fusion | flops 1677721600 | bytes 6881280 | tf_op jit(solution)/shard_map/dot_general | solution.py:167
  221.2 10.8 %convolution_convert_fusion.1 = bf16[640,2048]{1,0:T(8,128)(2,1)} fusion(bf16[640,2048]{0,1:T(8,128)(2,1)S(1)} %bitcast.215, f32[640,640]{1,0:T(8,128)} %fusion.15, bf16[640,2048]{1,0:T(8,128)(2,1)} %bitcast.218, bf16[2048,1280]{1,0:T(8,128)(2,1)} %all-gather.3.cloned.1.call-done), kind=kOutput, calls=%fused_computation.27 | convolution fusion | flops 3359211520 | bytes 12124160 | tf_op jit(solution)/shard_map/dot_general | solution.py:65
  232.0 10.1 %all-to-all-start.2 = ((bf16[8,80,2048]{2,1,0:T(8,128)(2,1)}), bf16[8,80,2048]{2,1,0:T(8,128)(2,1)S(1)}, u32[]{:S(2)}, u32[]{:S(2)}) async-start(bf16[8,80,2048]{2,1,0:T(8,128)(2,1)} %bitcast.219), calls=%async_computation.2 | async-start | bytes 5242880 | tf_op jit(solution)/shard_map/all_to_all | solution.py:38
  243.2 30.7 %all-to-all-done.2 = bf16[8,80,2048]{2,1,0:T(8,128)(2,1)S(1)} async-done(((bf16[8,80,2048]{2,1,0:T(8,128)(2,1)}), bf16[8,80,2048]{2,1,0:T(8,128)(2,1)S(1)}, u32[]{:S(2)}, u32[]{:S(2)}) %all-to-all-start.2) | async-done | bytes 2621472 | tf_op jit(solution)/shard_map/all_to_all | solution.py:38
  275.1 1.9 broadcast_in_dim.67
  276.9 4.6 all-to-all-start.3
  281.7 31.8 %all-to-all-done.3 = bf16[8,80,2048]{2,1,0:T(8,128)(2,1)S(1)} async-done(((bf16[8,80,2048]{2,1,0:T(8,128)(2,1)}), bf16[8,80,2048]{2,1,0:T(8,128)(2,1)S(1)}, u32[]{:S(2)}, u32[]{:S(2)}) %all-to-all-start.3) | async-done | bytes 2621472 | tf_op jit(solution)/shard_map/all_to_all | solution.py:23
  314.4 7.8 %all-to-all-start.4 = ((bf16[16,128,128]{1,2,0:T(8,128)(2,1)}), bf16[16,128,128]{1,2,0:T(8,128)(2,1)}, u32[]{:S(2)}, u32[]{:S(2)}) async-start(bf16[16,128,128]{1,2,0:T(8,128)(2,1)} %broadcast_in_dim.69), calls=%async_computation.4 | async-start | bytes 1048576 | tf_op jit(solution)/shard_map/all_to_all | solution.py:23
  322.3 2.0 fusion.29
  325.2 2.0 fusion.28
  332.0 1.7 bitcast_subtract_fusion.3
  333.8 2.6 convolution_convert_fusion.4
  336.3 44.2 %while.41 = (s32[]{:T(128)}, f32[10,64,128]{2,1,0:T(8,128)}, f32[10,64,64]{2,1,0:T(8,128)}, f32[10,64,64]{2,1,0:T(8,128)}, f32[10,64,64]{2,1,0:T(8,128)S(1)}, /*...) while((s32[]{:T(128)}, f32[10,64,128]{2,1,0:T(8,128)}, ...), condition=%wide.region_6.7_spmd.clone, body=%wide.region_4.6_spmd.clone.sunk | while | flops 2621442 | bytes 271461 | solution.py:107
  382.4 1.9 convolution_bitcast_fusion.2
  384.3 1.9 convolution_bitcast_fusion.1
  386.9 7.9 %while.43 = (s32[]{:T(128)}, f32[2,1,64,128]{3,2,1,0:T(8,128)S(1)}, bf16[5,2,1,64,128]{4,3,1,2,0:T(8,128)(2,1)}, f32[5,2,1,64]{3,1,2,0:T(2,128)S(1)}, f32[5,2,1,...) while((s32[]{:T(128)}, f32[2,1,64,128]{3,2,1,0:T(8,128)S(1)}, ...), condition=%wide.region_10.11_spmd.clone, body=%wide.region_9.10_spmd.clone.sunk | while | flops 65540 | bytes 296576 | solution.py:130
  395.5 7.9 %while.42 = (s32[]{:T(128)}, f32[2,1,64,128]{3,2,1,0:T(8,128)S(1)}, bf16[5,2,1,64,128]{4,3,1,2,0:T(8,128)(2,1)}, f32[5,2,1,64]{3,1,2,0:T(2,128)S(1)}, f32[5,2,1,64,128]{4,3,1,2,0:T(8,128)}, /*index=5*/s32[]{:T(128)}, s32[]{:T(128)}) while((s32[]{:T(128)}, f32[2,1,64,128]{3,2,1,0:T(8,128)S(1)}, ...), condition=%wide.region_8.9_spmd.clone, body=%wide.region_7.8_spmd.clone.sunk | while | flops 65539 | bytes 296556 | solution.py:129
  404.6 2.2 multiply_reduce_fusion.4
  406.8 2.0 fusion.42
  408.8 1.9 convolution_convert_fusion.2
  410.7 35.6 %all_to_all.40 = bf16[8,80,2048]{2,1,0:T(8,128)(2,1)S(1)} all-to-all(bf16[8,80,2048]{2,1,0:T(8,128)(2,1)S(1)} %bitcast.203), channel_id=1, replica_groups=mesh['grp'=2,'fs'=16,'tp'=8] {'tp'}, dimensions={0} | all-to-all | bytes 5242880 | tf_op jit(solution)/shard_map/all_to_all | solution.py:38
  447.6 35.5 %all_to_all.41 = bf16[8,80,2048]{2,1,0:T(8,128)(2,1)S(1)} all-to-all(bf16[8,80,2048]{2,1,0:T(8,128)(2,1)S(1)} %broadcast_in_dim.70), channel_id=1, replica_groups=mesh['grp'=2,'fs'=16,'tp'=8] {'tp'}, dimensions={0} | all-to-all | bytes 5242880 | tf_op jit(solution)/shard_map/all_to_all | solution.py:23
  483.1 1.5 copy-done.5
  484.7 3.4 fusion.13
  488.1 9.7 %convolution_convert_fusion = bf16[640,2048]{1,0:T(8,128)(2,1)} fusion(bf16[640,2048]{0,1:T(8,128)(2,1)S(1)} %bitcast.216, f32[640,640]{0,1:T(8,128)} %fusion.13, bf16[640,2048]{1,0:T(8,128)(2,1)} %bitcast.221, bf16[2048,1280]{1,0:T(8,128)(2,1)} %all-gather.3.cloned.1.call-done), kind=kOutput, calls=%fused_computation.26 | convolution fusion | flops 3359211520 | bytes 12124160 | tf_op jit(solution)/shard_map/dot_general | solution.py:65
  497.8 36.4 %all_to_all.42 = bf16[8,80,2048]{2,1,0:T(8,128)(2,1)S(1)} all-to-all(bf16[8,80,2048]{2,1,0:T(8,128)(2,1)} %bitcast.222), channel_id=1, replica_groups=mesh['grp'=2,'fs'=16,'tp'=8] {'tp'}, dimensions={0} | all-to-all | bytes 5242880 | tf_op jit(solution)/shard_map/all_to_all | solution.py:38
  (171 shorter events, 77.7 us)
Async XLA Ops:
  6.5 321.6 %copy-start = (bf16[2048,32]{0,1:T(8,128)(2,1)S(1)}, bf16[2048,32]{0,1:T(8,128)(2,1)}, u32[]{:S(2)}) copy-start(bf16[2048,32]{0,1:T(8,128)(2,1)} %param.28) | copy-start | bytes 393220
  9.4 24.1 %copy-start.7 = (bf16[128,640]{1,0:T(8,128)(2,1)S(1)}, bf16[128,640]{1,0:T(8,128)(2,1)}, u32[]{:S(2)}) copy-start(bf16[128,640]{1,0:T(8,128)(2,1)} %param.22) | copy-start | bytes 491524
  9.4 24.1 %copy-start.8 = (bf16[128,640]{1,0:T(8,128)(2,1)S(1)}, bf16[128,640]{1,0:T(8,128)(2,1)}, u32[]{:S(2)}) copy-start(bf16[128,640]{1,0:T(8,128)(2,1)} %param.21) | copy-start | bytes 491524
  9.4 24.9 %copy-start.9 = (bf16[640,128]{1,0:T(8,128)(2,1)S(1)}, bf16[640,128]{1,0:T(8,128)(2,1)}, u32[]{:S(2)}) copy-start(bf16[640,128]{1,0:T(8,128)(2,1)} %param.23) | copy-start | bytes 491524
  9.4 56.0 %all-to-all-start = ((bf16[8,80,2048]{2,1,0:T(8,128)(2,1)}), bf16[8,80,2048]{2,1,0:T(8,128)(2,1)S(1)}, u32[]{:S(2)}, u32[]{:S(2)}) async-start(bf16[8,80,2048]{2,1,0:T(8,128)(2,1)} %broadcast_in_dim.65), calls=%async_computation | async-start | bytes 5242880 | tf_op jit(solution)/shard_map/all_to_all | solution.py:23
  33.5 181.8 %all-gather.3.cloned.1.call-start = ((), (), s32[]{:S(2)}) async-start(), calls=%async_computation.8 | async-start | bytes 5570560 | tf_op jit(solution)/shard_map/all_gather | solution.py:44
  65.4 2.4 copy-start.4
  67.7 153.4 %all-to-all-start.1 = ((bf16[16,640,128]{1,2,0:T(8,128)(2,1)}), bf16[16,640,128]{1,2,0:T(8,128)(2,1)S(1)}, u32[]{:S(2)}, u32[]{:S(2)}) async-start(bf16[16,640,128]{1,2,0:T(8,128)(2,1)} %stack.2), calls=%async_computation.1 | async-start | bytes 5242880 | tf_op jit(solution)/shard_map/all_to_all | solution.py:159
  221.2 10.8 %copy-start.2 = (bf16[16,640,128]{1,2,0:T(8,128)(2,1)}, bf16[16,640,128]{1,2,0:T(8,128)(2,1)S(1)}, u32[]{:S(2)}) copy-start(bf16[16,640,128]{1,2,0:T(8,128)(2,1)S(1)} %all-to-all-done.1) | copy-start | bytes 7864324
  232.0 10.1 %copy-start.13 = (bf16[128,64]{0,1:T(8,128)(2,1)S(1)}, bf16[128,64]{0,1:T(8,128)(2,1)}, u32[]{:S(2)}) copy-start(bf16[128,64]{0,1:T(8,128)(2,1)} %param.25) | copy-start | bytes 49156
  232.0 10.3 %copy-start.14 = (bf16[128,64]{0,1:T(8,128)(2,1)S(1)}, bf16[128,64]{0,1:T(8,128)(2,1)}, u32[]{:S(2)}) copy-start(bf16[128,64]{0,1:T(8,128)(2,1)} %param.24) | copy-start | bytes 49156
  232.0 10.4 %copy-start.10 = (bf16[128,128]{1,0:T(8,128)(2,1)S(1)}, bf16[128,128]{1,0:T(8,128)(2,1)}, u32[]{:S(2)}) copy-start(bf16[128,128]{1,0:T(8,128)(2,1)} %param.27) | copy-start | bytes 98308
  232.0 10.4 %copy-start.11 = (bf16[128,128]{1,0:T(8,128)(2,1)S(1)}, bf16[128,128]{1,0:T(8,128)(2,1)}, u32[]{:S(2)}) copy-start(bf16[128,128]{1,0:T(8,128)(2,1)} %param.26) | copy-start | bytes 98308
  232.0 41.9 %all-to-all-start.2 = ((bf16[8,80,2048]{2,1,0:T(8,128)(2,1)}), bf16[8,80,2048]{2,1,0:T(8,128)(2,1)S(1)}, u32[]{:S(2)}, u32[]{:S(2)}) async-start(bf16[8,80,2048]{2,1,0:T(8,128)(2,1)} %bitcast.219), calls=%async_computation.2 | async-start | bytes 5242880 | tf_op jit(solution)/shard_map/all_to_all | solution.py:38
  242.1 32.3 %copy-start.1 = (bf16[80,2048]{1,0:T(8,128)(2,1)S(1)}, bf16[80,2048]{1,0:T(8,128)(2,1)}, u32[]{:S(2)}) copy-start(bf16[80,2048]{1,0:T(8,128)(2,1)} %param.20) | copy-start | bytes 983044
  242.1 80.2 %all-gather.5.cloned.1.call-start = ((), (), s32[]{:S(2)}) async-start(), calls=%async_computation.9 | async-start | bytes 1671168 | tf_op jit(solution)/shard_map/all_gather | solution.py:44
  276.9 4.7 copy-start.12
  276.9 36.6 %all-to-all-start.3 = ((bf16[8,80,2048]{2,1,0:T(8,128)(2,1)}), bf16[8,80,2048]{2,1,0:T(8,128)(2,1)S(1)}, u32[]{:S(2)}, u32[]{:S(2)}) async-start(bf16[8,80,2048]{2,1,0:T(8,128)(2,1)} %broadcast_in_dim.67), calls=%async_computation.3 | async-start | bytes 5242880 | tf_op jit(solution)/shard_map/all_to_all | solution.py:23
  314.4 94.4 %all-to-all-start.4 = ((bf16[16,128,128]{1,2,0:T(8,128)(2,1)}), bf16[16,128,128]{1,2,0:T(8,128)(2,1)}, u32[]{:S(2)}, u32[]{:S(2)}) async-start(bf16[16,128,128]{1,2,0:T(8,128)(2,1)} %broadcast_in_dim.69), calls=%async_computation.4 | async-start | bytes 1048576 | tf_op jit(solution)/shard_map/all_to_all | solution.py:23
  324.2 3.9 copy-start.6
  324.3 3.9 copy-start.15
  324.3 3.9 copy-start.16
  394.8 12.0 %copy-start.17 = (f32[128]{0:T(128)S(1)}, f32[128]{0:T(128)}, u32[]{:S(2)}) copy-start(f32[128]{0:T(128)} %param.32) | copy-start | bytes 1540
  446.7 38.0 %slice-start = ((s8[5242880]{0:T(1024)(128)(4,1)}), s8[4194304]{0:T(1024)(128)(4,1)S(1)}, s32[]{:S(2)}) async-start(s8[5242880]{0:T(1024)(128)(4,1)} %bitcast.230), calls=%async_computation.10 | async-start | bytes 8388608
  447.3 37.4 %slice-start.1 = ((s8[5242880]{0:T(1024)(128)(4,1)}), s8[1048576]{0:T(1024)(128)(4,1)S(1)}, s32[]{:S(2)}) async-start(s8[5242880]{0:T(1024)(128)(4,1)} %bitcast.230), calls=%async_computation.11 | async-start | bytes 2097152
  483.1 1.5 copy-start.5
  484.7 3.4 copy-start.3
Sparse Core Ops, SparseCore 0:
  36.1 179.1 all-gather.2
  244.7 57.4 all-gather.4
